TPU v7x, 512 devices: a whole 4x4x16 slice. The times are simulated.
512 devices in a mesh: ra: 16 (over z), cb: 4 (over y), dp: 8 (over x, core).
Axes of the slice: x: 4, y: 4, z: 16, core: 2. Of those that a mesh axis runs over, the one named last changes fastest.
Arguments:
- tokens: bfloat16 [8, 512, 4096], P('dp', None, 'ra'), may hold values from -80 to 80
- pre_gain: float32 [4096], P('ra'), may hold values from 0.1 to 1.9
- w_gate: bfloat16 [4096, 11264], P('ra', 'cb'), may hold values from -0.09375 to 0.09375
- w_up: bfloat16 [4096, 11264], P('ra', 'cb'), may hold values from -0.09375 to 0.09375
- conv_gate: float32 [3, 11264], P(None, 'cb'), may hold values from -3.5 to 3.5
- conv_up: float32 [3, 11264], P(None, 'cb'), may hold values from -3.5 to 3.5
- w_down: bfloat16 [11264, 4096], P('cb', 'ra'), may hold values from -2 to 2
- post_gain: float32 [4096], P('ra'), may hold values from 0.1 to 1.9
Outputs:
- mixed: bfloat16 [8, 512, 4096], P('dp', None, 'ra')
All inputs are finite; a program needn't handle non-finite values.
Results may differ from a plain program's by a relative error of at most 0.0064.
Values may be sent and summed in bfloat16 or wider, within the bound.
A program may use at most 64 MiB of HBM per device.

v0:
```python
import jax
import jax.numpy as jnp
from jax import lax
from jax.sharding import PartitionSpec as P

epsilon = 1e-06
residual_scale = 0.125


def from_everyone(array, axis):
    count = lax.axis_size(axis)
    return lax.all_to_all(
        jnp.broadcast_to(array[None], (count, *array.shape)), axis, 0, 0, tiled=True
    )


def over_copies(array, axis):
    return from_everyone(array, axis).sum(axis=0)


def split_up(array, dim, count):
    dims = array.shape
    tiles = array.reshape(*dims[:dim], count, dims[dim] // count, *dims[dim + 1 :])
    return jnp.moveaxis(tiles, dim, 0)


def summed_on_arrival(array, axis, dim):
    count = lax.axis_size(axis)
    tiles = lax.all_to_all(split_up(array, dim, count), axis, 0, 0, tiled=True)
    return jnp.sum(tiles, axis=0)


def convolve(field, tap_weights):
    zero_col = jnp.zeros((field.shape[0], 1), jnp.float32)
    before = jnp.concatenate([zero_col, field[:, :-1]], axis=1)
    later_cols = jnp.concatenate([field[:, 1:], zero_col], axis=1)
    return (
        tap_weights[0][:, None] * before
        + tap_weights[1][:, None] * field
        + tap_weights[2][:, None] * later_cols
    )


def local(tokens, pre_gain, w_gate, w_up, conv_gate, conv_up, w_down, post_gain):
    ra_count = lax.axis_size("ra")
    dim_full = tokens.shape[2] * ra_count
    values = tokens[0].astype(jnp.float32)
    local_sq = jnp.sum(values * values, axis=1)
    total_sq = over_copies(local_sq, "ra")
    in_scale = lax.rsqrt(total_sq / dim_full + epsilon)
    weighted = (values * pre_gain).astype(jnp.bfloat16)
    gate_cols, up_cols = (
        lax.all_to_all(w_gate, "ra", split_axis=1, concat_axis=0, tiled=True),
        lax.all_to_all(w_up, "ra", split_axis=1, concat_axis=0, tiled=True),
    )
    own_units = gate_cols.shape[1]
    piece = lax.all_gather(weighted, "ra", axis=1, tiled=True)
    dims = (((0,), (1,)), ((), ()))
    gate_sum = lax.dot_general(gate_cols, piece, dims, preferred_element_type=jnp.float32)
    up_sum = lax.dot_general(up_cols, piece, dims, preferred_element_type=jnp.float32)
    offset_units = lax.axis_index("ra") * own_units
    taps_gate = lax.dynamic_slice_in_dim(conv_gate, offset_units, own_units, 1)
    taps_up = lax.dynamic_slice_in_dim(conv_up, offset_units, own_units, 1)
    gate_lin = gate_sum * in_scale[None, :]
    up_lin = up_sum * in_scale[None, :]
    hidden = (
        jax.nn.gelu(convolve(gate_lin, taps_gate), approximate=True) * convolve(up_lin, taps_up)
    ).astype(jnp.bfloat16)
    partial_value = lax.dot_general(
        lax.all_gather(hidden, "ra", axis=0, tiled=True),
        w_down,
        (((0,), (0,)), ((), ())),
        preferred_element_type=jnp.float32,
    )
    share = summed_on_arrival(partial_value, "cb", 1)
    share_cols = share.shape[1]
    col_start = lax.axis_index("cb") * share_cols
    own_values = lax.dynamic_slice_in_dim(values, col_start, share_cols, 1)
    own_gain = lax.dynamic_slice_in_dim(post_gain, col_start, share_cols, 0)
    post_sq = over_copies(jnp.sum(share * share, axis=1), ("ra", "cb"))
    post_scale = lax.rsqrt(post_sq / dim_full + epsilon)
    mixed_part = (residual_scale * own_values + share * post_scale[:, None] * own_gain).astype(
        jnp.bfloat16
    )
    mixed = lax.all_gather(mixed_part, "cb", axis=1, tiled=True)
    return mixed[None]


def solution(mesh):
    in_specs = (
        P("dp", None, "ra"),
        P("ra"),
        P("ra", "cb"),
        P("ra", "cb"),
        P(None, "cb"),
        P(None, "cb"),
        P("cb", "ra"),
        P("ra"),
    )
    out_specs = P("dp", None, "ra")
    return jax.shard_map(local, mesh=mesh, in_specs=in_specs, out_specs=out_specs, check_vma=False)
```

profile of v0, /device:TPU:2, one launch (start us, length us, event | category | flops | bytes accessed | tf_op | source)
XLA Modules:
  0.0 356.9 jit_solution(16461781965745227600)
XLA Ops:
  6.5 1.2 copy.25
  7.7 1.5 fusion.3
  9.2 0.6 broadcast_in_dim.6
  9.9 15.2 %all-to-all-start.1 = ((f32[16,1,512]{2,1,0:T(1,128)}), f32[16,1,512]{2,1,0:T(1,128)S(1)}, u32[]{:S(2)}, u32[]{:S(2)}) async-start(f32[16,1,512]{2,1,0:T(1,128)} %broadcast_in_dim.6), calls=%async_computation.1 | async-start | bytes 65536 | tf_op jit(solution)/shard_map/all_to_all | solution.py:12
  25.1 2.5 copy.29
  27.6 10.0 %all-to-all-done.1 = f32[16,1,512]{2,1,0:T(1,128)S(1)} async-done(((f32[16,1,512]{2,1,0:T(1,128)}), f32[16,1,512]{2,1,0:T(1,128)S(1)}, u32[]{:S(2)}, u32[]{:S(2)}) %all-to-all-start.1) | async-done | bytes 32800 | tf_op jit(solution)/shard_map/all_to_all | solution.py:12
  37.6 3.7 %all-to-all-start.2 = ((bf16[256,16,176]{0,2,1:T(8,128)(2,1)}), bf16[256,16,176]{0,2,1:T(8,128)(2,1)S(1)}, u32[]{:S(2)}, u32[]{:S(2)}) async-start(bf16[256,16,176]{0,2,1:T(8,128)(2,1)} %bitcast.41), calls=%async_computation.2 | async-start | bytes 2883584 | tf_op jit(solution)/shard_map/all_to_all | solution.py:54
  41.4 0.7 all-gather.3.cloned.1.call-update
  42.1 2.5 copy.26
  44.6 72.1 %all-to-all-done.2 = bf16[256,16,176]{0,2,1:T(8,128)(2,1)S(1)} async-done(((bf16[256,16,176]{0,2,1:T(8,128)(2,1)}), bf16[256,16,176]{0,2,1:T(8,128)(2,1)S(1)}, u32[]{:S(2)}, u32[]{:S(2)}) %all-to-all-start.2) | async-done | bytes 1441824 | tf_op jit(solution)/shard_map/all_to_all | solution.py:54
  116.7 10.3 %all-to-all-start = ((bf16[256,16,176]{0,2,1:T(8,128)(2,1)}), bf16[256,16,176]{0,2,1:T(8,128)(2,1)}, u32[]{:S(2)}, u32[]{:S(2)}) async-start(bf16[256,16,176]{0,2,1:T(8,128)(2,1)} %bitcast.40), calls=%async_computation | async-start | bytes 2883584 | tf_op jit(solution)/shard_map/all_to_all | solution.py:53
  127.1 0.9 constant_dynamic-slice_fusion
  128.0 1.3 copy.36
  129.3 78.8 %all-to-all-done = bf16[256,16,176]{0,2,1:T(8,128)(2,1)} async-done(((bf16[256,16,176]{0,2,1:T(8,128)(2,1)}), bf16[256,16,176]{0,2,1:T(8,128)(2,1)}, u32[]{:S(2)}, u32[]{:S(2)}) %all-to-all-start) | async-done | bytes 1441824 | tf_op jit(solution)/shard_map/all_to_all | solution.py:53
  208.2 2.8 copy.35
  210.9 5.6 %all-gather.3.cloned.1.call-done = bf16[512,4096]{0,1:T(8,128)(2,1)} async-done(((bf16[512,256]{0,1:T(8,128)(2,1)}), bf16[512,4096]{0,1:T(8,128)(2,1)}) %all-gather.3.cloned.1.call-update) | async-done | bytes 4194320 | tf_op jit(solution)/shard_map/all_gather | solution.py:57
  216.5 3.3 fusion.1
  219.8 0.2 copy-done.1
  220.0 0.4 copy-done.3
  220.4 0.9 fusion
  221.3 0.3 fusion.14
  221.6 1.2 fusion.12
  222.8 72.5 %all-gather.5.cloned.1.call-done = bf16[2816,512]{1,0:T(8,128)(2,1)} async-done(((bf16[176,512]{1,0:T(8,128)(2,1)}), bf16[2816,512]{1,0:T(8,128)(2,1)}) %all-gather.5.cloned.1.call-update) | async-done | bytes 2883600 | tf_op jit(solution)/shard_map/all_gather | solution.py:70
  295.4 2.8 fusion.16
  298.1 12.2 %all_to_all.55 = f32[4,512,64]{1,2,0:T(8,128)S(1)} all-to-all(f32[4,512,64]{1,2,0:T(8,128)S(1)} %bitcast.45), channel_id=1, replica_groups=mesh['ra'=16,'cb'=4,'dp'=8] {'cb'}, dimensions={0} | all-to-all | bytes 1048576 | tf_op jit(solution)/shard_map/all_to_all | solution.py:29
  310.4 0.7 broadcast_in_dim.7
  311.2 9.4 %all-to-all-start.4 = ((f32[64,1,512]{2,1,0:T(1,128)}), f32[64,1,512]{2,1,0:T(1,128)S(1)}, u32[]{:S(2)}, u32[]{:S(2)}) async-start(f32[64,1,512]{2,1,0:T(1,128)} %broadcast_in_dim.7), calls=%async_computation.4 | async-start | bytes 262144 | tf_op jit(solution)/shard_map/all_to_all | solution.py:12
  320.7 16.0 %all-to-all-done.4 = f32[64,1,512]{2,1,0:T(1,128)S(1)} async-done(((f32[64,1,512]{2,1,0:T(1,128)}), f32[64,1,512]{2,1,0:T(1,128)S(1)}, u32[]{:S(2)}, u32[]{:S(2)}) %all-to-all-start.4) | async-done | bytes 131104 | tf_op jit(solution)/shard_map/all_to_all | solution.py:12
  336.7 0.1 reduce_sum.49
  336.8 0.1 fusion.13
  336.9 12.3 %all_gather.11 = bf16[512,256]{0,1:T(8,128)(2,1)S(1)} all-gather(bf16[512,64]{0,1:T(8,128)(2,1)S(1)} %fusion.13), channel_id=1, replica_groups=mesh['ra'=16,'cb'=4,'dp'=8] {'cb'}, dimensions={1}, use_global_device_ids=true | all-gather | bytes 327680 | tf_op jit(solution)/shard_map/all_gather | solution.py:85
  349.2 0.8 copy.32
  (18 shorter events, 0.4 us)
Async XLA Ops:
  6.5 288.8 %copy-start = (bf16[2816,256]{1,0:T(8,128)(2,1)S(1)}, bf16[2816,256]{1,0:T(8,128)(2,1)}, u32[]{:S(2)}) copy-start(bf16[2816,256]{1,0:T(8,128)(2,1)} %param.14) | copy-start | bytes 4325380
  9.9 27.8 %all-to-all-start.1 = ((f32[16,1,512]{2,1,0:T(1,128)}), f32[16,1,512]{2,1,0:T(1,128)S(1)}, u32[]{:S(2)}, u32[]{:S(2)}) async-start(f32[16,1,512]{2,1,0:T(1,128)} %broadcast_in_dim.6), calls=%async_computation.1 | async-start | bytes 65536 | tf_op jit(solution)/shard_map/all_to_all | solution.py:12
  37.6 79.1 %all-to-all-start.2 = ((bf16[256,16,176]{0,2,1:T(8,128)(2,1)}), bf16[256,16,176]{0,2,1:T(8,128)(2,1)S(1)}, u32[]{:S(2)}, u32[]{:S(2)}) async-start(bf16[256,16,176]{0,2,1:T(8,128)(2,1)} %bitcast.41), calls=%async_computation.2 | async-start | bytes 2883584 | tf_op jit(solution)/shard_map/all_to_all | solution.py:54
  41.3 175.2 %all-gather.3.cloned.1.call-start = ((), (), s32[]{:S(2)}) async-start(), calls=%async_computation.5 | async-start | bytes 4456448 | tf_op jit(solution)/shard_map/all_gather | solution.py:57
  116.7 91.4 %all-to-all-start = ((bf16[256,16,176]{0,2,1:T(8,128)(2,1)}), bf16[256,16,176]{0,2,1:T(8,128)(2,1)}, u32[]{:S(2)}, u32[]{:S(2)}) async-start(bf16[256,16,176]{0,2,1:T(8,128)(2,1)} %bitcast.40), calls=%async_computation | async-start | bytes 2883584 | tf_op jit(solution)/shard_map/all_to_all | solution.py:53
  127.0 168.3 %all-gather.5.cloned.1.call-start = ((), (), s32[]{:S(2)}) async-start(), calls=%async_computation.6 | async-start | bytes 3063808 | tf_op jit(solution)/shard_map/all_gather | solution.py:70
  208.2 8.4 %copy-start.2 = (bf16[16,22,8,256]{3,2,0,1:T(8,128)(2,1)S(1)}, bf16[16,22,8,256]{3,2,0,1:T(8,128)(2,1)}, u32[]{:S(2)}) copy-start(bf16[16,22,8,256]{3,2,0,1:T(8,128)(2,1)} %copy.36) | copy-start | bytes 4325380
  216.5 3.4 copy-start.1
  216.5 3.9 %copy-start.3 = (bf16[16,22,8,256]{3,2,0,1:T(8,128)(2,1)S(1)}, bf16[16,22,8,256]{3,2,0,1:T(8,128)(2,1)}, u32[]{:S(2)}) copy-start(bf16[16,22,8,256]{3,2,0,1:T(8,128)(2,1)} %copy.35) | copy-start | bytes 4325380
  298.1 22.5 %copy-start.4 = (f32[256]{0:T(256)S(1)}, f32[256]{0:T(256)}, u32[]{:S(2)}) copy-start(f32[256]{0:T(256)} %param.15) | copy-start | bytes 3076
  311.2 25.6 %all-to-all-start.4 = ((f32[64,1,512]{2,1,0:T(1,128)}), f32[64,1,512]{2,1,0:T(1,128)S(1)}, u32[]{:S(2)}, u32[]{:S(2)}) async-start(f32[64,1,512]{2,1,0:T(1,128)} %broadcast_in_dim.7), calls=%async_computation.4 | async-start | bytes 262144 | tf_op jit(solution)/shard_map/all_to_all | solution.py:12
Sparse Core Ops, SparseCore 0:
  44.2 172.2 all-gather.2
  222.9 72.3 all-gather.4
where the time goes:
time: 357 us
  waiting for transfers between devices  256 us (72%)
  starting transfers between devices  38.7 us (11%)
  blocking collectives  24.5 us (7%)
  local copies, waits for them, and re-layouts  14.4 us (4%)
  between operations  13.5 us (4%)
  matrix products  6.94 us (2%)
    all_to_all x1, waiting for transfers between devices, local(): lax.all_to_all(w_gate, 'ra', split_axis=1, concat_axis=0, tiled=True)  78.8 us
    all_gather x1, waiting for transfers between devices, local(): lax.all_gather(hidden, 'ra', axis=0, tiled=True)  72.5 us
    all_to_all x1, waiting for transfers between devices, local(): lax.all_to_all(w_up, 'ra', split_axis=1, concat_axis=0, tiled=True)  72.1 us
    all_to_all x2, waiting for transfers between devices, from_everyone(): lax.all_to_all(jnp.broadcast_to(array[None], (count, *array.shape)), axis...  26 us
    all_to_all x2, starting transfers between devices, from_everyone(): lax.all_to_all(jnp.broadcast_to(array[None], (count, *array.shape)), axis...  24.6 us
    all_gather x1, blocking collectives, local(): mixed = lax.all_gather(mixed_part, 'cb', axis=1, tiled=True)  12.3 us
    all_to_all x1, blocking collectives, summed_on_arrival(): tiles = lax.all_to_all(split_up(array, dim, count), axis, 0, 0, tiled=True)  12.2 us
    all_to_all x1, starting transfers between devices, local(): lax.all_to_all(w_gate, 'ra', split_axis=1, concat_axis=0, tiled=True)  10.3 us
  transfers between devices with their start and end apart: 6, of which 6 were waited for; matrix products, arithmetic and copies ran while one was open for 3% of the time, Pallas kernels for 0%

commit v1 on v0

--- a/solution.py
+++ b/solution.py
@@ -5,6 +5,28 @@
 
 epsilon = 1e-06
 residual_scale = 0.125
+
+
+def joined_along(blocks, dim):
+    lengths = list(blocks.shape[1:])
+    lengths[dim] *= blocks.shape[0]
+    return jnp.moveaxis(blocks, 0, dim).reshape(lengths)
+
+
+def collect(x, axis, dim):
+    length = lax.axis_size(axis)
+    pairs = [(i, (i + 1) % length) for i in range(length)]
+    back = [(b, a) for a, b in pairs]
+    lower, upper = ([], [])
+    for lap in range(length - 1):
+        if lap % 2 == 0:
+            lower.append(lax.ppermute(lower[-1] if lower else x, axis, pairs))
+        else:
+            upper.append(lax.ppermute(upper[-1] if upper else x, axis, back))
+    blocks = jnp.stack([*lower[::-1], x, *upper])
+    shift = lax.axis_index(axis) - len(lower)
+    blocks = blocks[(jnp.arange(length) - shift) % length]
+    return joined_along(blocks, dim)
 
 
 def from_everyone(array, axis):
@@ -67,7 +89,7 @@
         jax.nn.gelu(convolve(gate_lin, taps_gate), approximate=True) * convolve(up_lin, taps_up)
     ).astype(jnp.bfloat16)
     partial_value = lax.dot_general(
-        lax.all_gather(hidden, "ra", axis=0, tiled=True),
+        collect(hidden, "ra", 0),
         w_down,
         (((0,), (0,)), ((), ())),
         preferred_element_type=jnp.float32,

time: 357 us -> 367 us (1.028)
  starting transfers between devices: 38.7 us -> 91.9 us
  waiting for transfers between devices: 256 us -> 204 us
  local copies, waits for them, and re-layouts: 14.4 us -> 22 us
    all_gather x1 -> x0, waiting for transfers between devices: 72.5 us -> none  [local(): lax.all_gather(hidden, 'ra', axis=0, tiled=True)]
    ppermute x0 -> x15, starting transfers between devices: none -> 52.7 us  [the longest x7 34.3 us: collect(): upper.append(lax.ppermute(upper[-1] if upper else x, axis, back))]
    ppermute x0 -> x15, waiting for transfers between devices: none -> 18.8 us  [the longest x8 17 us: collect(): lower.append(lax.ppermute(lower[-1] if lower else x, axis, pairs))]
    unnamed x13 -> x59, local copies, waits for them, and re-layouts: 6.93 us -> 13.5 us
  transfers between devices with their start and end apart: 6 -> 20, of which waited for: 6 -> 15; matrix products, arithmetic and copies ran while one was open for 3% -> 4% of each run, Pallas kernels for 0% -> 0%
where the time goes in v1:
time: 367 us; the launch traced here: 366 us
  waiting for transfers between devices  204 us (56%)
  starting transfers between devices  91.9 us (25%)
  blocking collectives  24.5 us (7%)
  local copies, waits for them, and re-layouts  22 us (6%)
  between operations  14 us (4%)
  matrix products  7.29 us (2%)
    all_to_all x1, waiting for transfers between devices, local(): lax.all_to_all(w_gate, 'ra', split_axis=1, concat_axis=0, tiled=True)  78.7 us
    all_to_all x1, waiting for transfers between devices, local(): lax.all_to_all(w_up, 'ra', split_axis=1, concat_axis=0, tiled=True)  73.1 us
    ppermute x7, starting transfers between devices, collect(): upper.append(lax.ppermute(upper[-1] if upper else x, axis, back))  34.3 us
    all_to_all x2, waiting for transfers between devices, from_everyone(): lax.all_to_all(jnp.broadcast_to(array[None], (count, *array.shape)), axis...  25.9 us
    all_to_all x2, starting transfers between devices, from_everyone(): lax.all_to_all(jnp.broadcast_to(array[None], (count, *array.shape)), axis...  25.2 us
    ppermute x8, starting transfers between devices, collect(): lower.append(lax.ppermute(lower[-1] if lower else x, axis, pairs))  18.4 us
    ppermute x8, waiting for transfers between devices, collect(): lower.append(lax.ppermute(lower[-1] if lower else x, axis, pairs))  17 us
    unnamed x59, local copies, waits for them, and re-layouts  13.5 us
  transfers between devices with their start and end apart: 20, of which 15 were waited for; matrix products, arithmetic and copies ran while one was open for 4% of the time, Pallas kernels for 0%

profile of v1, /device:TPU:2, one launch (start us, length us, event | category | flops | bytes accessed | tf_op | source)
XLA Modules:
  0.0 366.4 jit_solution(5583362391558895906)
XLA Ops:
  9.8 15.2 %all-to-all-start.1 = ((f32[16,1,512]{2,1,0:T(1,128)}), f32[16,1,512]{2,1,0:T(1,128)S(1)}, u32[]{:S(2)}, u32[]{:S(2)}) async-start(f32[16,1,512]{2,1,0:T(1,128)} %broadcast_in_dim.6), calls=%async_computation.1 | async-start | bytes 65536 | tf_op jit(solution)/shard_map/all_to_all | solution.py:34
  25.0 2.7 copy.33
  27.6 9.9 %all-to-all-done.1 = f32[16,1,512]{2,1,0:T(1,128)S(1)} async-done(((f32[16,1,512]{2,1,0:T(1,128)}), f32[16,1,512]{2,1,0:T(1,128)S(1)}, u32[]{:S(2)}, u32[]{:S(2)}) %all-to-all-start.1) | async-done | bytes 32800 | tf_op jit(solution)/shard_map/all_to_all | solution.py:34
  37.5 3.7 %all-to-all-start.2 = ((bf16[256,16,176]{0,2,1:T(8,128)(2,1)}), bf16[256,16,176]{0,2,1:T(8,128)(2,1)S(1)}, u32[]{:S(2)}, u32[]{:S(2)}) async-start(bf16[256,16,176]{0,2,1:T(8,128)(2,1)} %bitcast.9), calls=%async_computation.2 | async-start | bytes 2883584 | tf_op jit(solution)/shard_map/all_to_all | solution.py:76
  43.5 73.1 %all-to-all-done.2 = bf16[256,16,176]{0,2,1:T(8,128)(2,1)S(1)} async-done(((bf16[256,16,176]{0,2,1:T(8,128)(2,1)}), bf16[256,16,176]{0,2,1:T(8,128)(2,1)S(1)}, u32[]{:S(2)}, u32[]{:S(2)}) %all-to-all-start.2) | async-done | bytes 1441824 | tf_op jit(solution)/shard_map/all_to_all | solution.py:76
  116.6 10.2 %all-to-all-start = ((bf16[256,16,176]{0,2,1:T(8,128)(2,1)}), bf16[256,16,176]{0,2,1:T(8,128)(2,1)S(1)}, u32[]{:S(2)}, u32[]{:S(2)}) async-start(bf16[256,16,176]{0,2,1:T(8,128)(2,1)} %bitcast.3), calls=%async_computation | async-start | bytes 2883584 | tf_op jit(solution)/shard_map/all_to_all | solution.py:75
  129.2 78.7 %all-to-all-done = bf16[256,16,176]{0,2,1:T(8,128)(2,1)S(1)} async-done(((bf16[256,16,176]{0,2,1:T(8,128)(2,1)}), bf16[256,16,176]{0,2,1:T(8,128)(2,1)S(1)}, u32[]{:S(2)}, u32[]{:S(2)}) %all-to-all-start) | async-done | bytes 1441824 | tf_op jit(solution)/shard_map/all_to_all | solution.py:75
  209.3 7.2 %all-gather.2.cloned.1.call-done = bf16[512,4096]{0,1:T(8,128)(2,1)} async-done(((bf16[512,256]{0,1:T(8,128)(2,1)}), bf16[512,4096]{0,1:T(8,128)(2,1)}) %all-gather.2.cloned.1.call-update) | async-done | bytes 4194320 | tf_op jit(solution)/shard_map/all_gather | solution.py:79
  216.4 3.3 fusion.1
  222.0 3.5 collective-permute-start
  225.5 5.1 %collective-permute-done = bf16[176,512]{1,0:T(8,128)(2,1)S(1)} collective-permute-done((bf16[176,512]{1,0:T(8,128)(2,1)S(1)}, bf16[176,512]{1,0:T(8,128)(2,1)S(1)}, u32[]{:S(2)}, u32[]{:S(2)}) %collective-permute-start) | collective-permute-done | bytes 180256 | tf_op jit(solution)/shard_map/ppermute | solution.py:23
  230.6 2.2 collective-permute-start.1
  232.9 4.8 %collective-permute-start.8 = (bf16[176,512]{1,0:T(8,128)(2,1)S(1)}, bf16[176,512]{1,0:T(8,128)(2,1)S(1)}, u32[]{:S(2)}, u32[]{:S(2)}) collective-permute-start(bf16[176,512]{1,0:T(8,128)(2,1)S(1)} %fusion.12), channel_id=1, source_target_pairs={{32,0},{64,32},{96,64},{128,96},{160,128},{192,160},{224,192},{256... | collective-permute-start | bytes 540680 | tf_op jit(solution)/shard_map/ppermute | solution.py:25
  239.2 2.8 collective-permute-start.2
  242.0 4.2 %collective-permute-start.9 = (bf16[176,512]{1,0:T(8,128)(2,1)S(1)}, bf16[176,512]{1,0:T(8,128)(2,1)S(1)}, u32[]{:S(2)}, u32[]{:S(2)}) collective-permute-start(bf16[176,512]{1,0:T(8,128)(2,1)S(1)} %collective-permute-done.8), channel_id=1, source_target_pairs={{32,0},{64,32},{96,64},{128,96},{160,128},{192,160},{224,192},{256... | collective-permute-start | bytes 540680 | tf_op jit(solution)/shard_map/ppermute | solution.py:25
  246.3 2.3 collective-permute-done.2
  248.6 2.2 collective-permute-start.3
  251.6 4.3 %collective-permute-start.10 = (bf16[176,512]{1,0:T(8,128)(2,1)S(1)}, bf16[176,512]{1,0:T(8,128)(2,1)S(1)}, u32[]{:S(2)}, u32[]{:S(2)}) collective-permute-start(bf16[176,512]{1,0:T(8,128)(2,1)S(1)} %collective-permute-done.9), channel_id=1, source_target_pairs={{32,0},{64,32},{96,64},{128,96},{160,128},{192,160},{224,192},{256... | collective-permute-start | bytes 540680 | tf_op jit(solution)/shard_map/ppermute | solution.py:25
  255.9 3.2 collective-permute-done.3
  261.0 5.1 %collective-permute-start.11 = (bf16[176,512]{1,0:T(8,128)(2,1)S(1)}, bf16[176,512]{1,0:T(8,128)(2,1)S(1)}, u32[]{:S(2)}, u32[]{:S(2)}) collective-permute-start(bf16[176,512]{1,0:T(8,128)(2,1)S(1)} %collective-permute-done.10), channel_id=1, source_target_pairs={{32,0},{64,32},{96,64},{128,96},{160,128},{192,160},{224,192},{256... | collective-permute-start | bytes 540680 | tf_op jit(solution)/shard_map/ppermute | solution.py:25
  266.2 2.6 collective-permute-done.4
  268.8 1.9 collective-permute-start.5
  270.7 5.1 %collective-permute-start.12 = (bf16[176,512]{1,0:T(8,128)(2,1)S(1)}, bf16[176,512]{1,0:T(8,128)(2,1)S(1)}, u32[]{:S(2)}, u32[]{:S(2)}) collective-permute-start(bf16[176,512]{1,0:T(8,128)(2,1)S(1)} %collective-permute-done.11), channel_id=1, source_target_pairs={{32,0},{64,32},{96,64},{128,96},{160,128},{192,160},{224,192},{256... | collective-permute-start | bytes 540680 | tf_op jit(solution)/shard_map/ppermute | solution.py:25
  275.8 2.0 collective-permute-done.5
  281.5 5.1 %collective-permute-start.13 = (bf16[176,512]{1,0:T(8,128)(2,1)S(1)}, bf16[176,512]{1,0:T(8,128)(2,1)S(1)}, u32[]{:S(2)}, u32[]{:S(2)}) collective-permute-start(bf16[176,512]{1,0:T(8,128)(2,1)S(1)} %collective-permute-done.12), channel_id=1, source_target_pairs={{32,0},{64,32},{96,64},{128,96},{160,128},{192,160},{224,192},{256... | collective-permute-start | bytes 540680 | tf_op jit(solution)/shard_map/ppermute | solution.py:25
  289.8 5.6 %collective-permute-start.14 = (bf16[176,512]{1,0:T(8,128)(2,1)S(1)}, bf16[176,512]{1,0:T(8,128)(2,1)S(1)}, u32[]{:S(2)}, u32[]{:S(2)}) collective-permute-start(bf16[176,512]{1,0:T(8,128)(2,1)S(1)} %collective-permute-done.13), channel_id=1, source_target_pairs={{32,0},{64,32},{96,64},{128,96},{160,128},{192,160},{224,192},{256... | collective-permute-start | bytes 540680 | tf_op jit(solution)/shard_map/ppermute | solution.py:25
  301.6 2.3 gather_fusion
  303.9 3.1 convolution_bitcast_fusion
  307.0 12.2 %all_to_all.55 = f32[4,512,64]{1,2,0:T(8,128)S(1)} all-to-all(f32[4,512,64]{1,2,0:T(8,128)S(1)} %convolution_bitcast_fusion), channel_id=1, replica_groups=mesh['ra'=16,'cb'=4,'dp'=8] {'cb'}, dimensions={0} | all-to-all | bytes 1048576 | tf_op jit(solution)/shard_map/all_to_all | solution.py:51
  320.1 10.0 %all-to-all-start.4 = ((f32[64,1,512]{2,1,0:T(1,128)}), f32[64,1,512]{2,1,0:T(1,128)S(1)}, u32[]{:S(2)}, u32[]{:S(2)}) async-start(f32[64,1,512]{2,1,0:T(1,128)} %broadcast_in_dim.7), calls=%async_computation.4 | async-start | bytes 262144 | tf_op jit(solution)/shard_map/all_to_all | solution.py:34
  330.2 16.0 %all-to-all-done.4 = f32[64,1,512]{2,1,0:T(1,128)S(1)} async-done(((f32[64,1,512]{2,1,0:T(1,128)}), f32[64,1,512]{2,1,0:T(1,128)S(1)}, u32[]{:S(2)}, u32[]{:S(2)}) %all-to-all-start.4) | async-done | bytes 131104 | tf_op jit(solution)/shard_map/all_to_all | solution.py:34
  346.5 12.3 %all_gather.7 = bf16[512,256]{0,1:T(8,128)(2,1)S(1)} all-gather(bf16[512,64]{0,1:T(8,128)(2,1)S(1)} %fusion.13), channel_id=1, replica_groups=mesh['ra'=16,'cb'=4,'dp'=8] {'cb'}, dimensions={1}, use_global_device_ids=true | all-gather | bytes 327680 | tf_op jit(solution)/shard_map/all_gather | solution.py:107
  (95 shorter events, 30.4 us)
Async XLA Ops:
  9.8 27.8 %all-to-all-start.1 = ((f32[16,1,512]{2,1,0:T(1,128)}), f32[16,1,512]{2,1,0:T(1,128)S(1)}, u32[]{:S(2)}, u32[]{:S(2)}) async-start(f32[16,1,512]{2,1,0:T(1,128)} %broadcast_in_dim.6), calls=%async_computation.1 | async-start | bytes 65536 | tf_op jit(solution)/shard_map/all_to_all | solution.py:34
  25.0 17.0 %copy-start.3 = (bf16[256,2816]{1,0:T(8,128)(2,1)S(1)}, bf16[256,2816]{1,0:T(8,128)(2,1)}, u32[]{:S(2)}) copy-start(bf16[256,2816]{1,0:T(8,128)(2,1)} %param.10) | copy-start | bytes 4325380
  37.5 79.1 %all-to-all-start.2 = ((bf16[256,16,176]{0,2,1:T(8,128)(2,1)}), bf16[256,16,176]{0,2,1:T(8,128)(2,1)S(1)}, u32[]{:S(2)}, u32[]{:S(2)}) async-start(bf16[256,16,176]{0,2,1:T(8,128)(2,1)} %bitcast.9), calls=%async_computation.2 | async-start | bytes 2883584 | tf_op jit(solution)/shard_map/all_to_all | solution.py:76
  41.2 175.2 %all-gather.2.cloned.1.call-start = ((), (), s32[]{:S(2)}) async-start(), calls=%async_computation.5 | async-start | bytes 4456448 | tf_op jit(solution)/shard_map/all_gather | solution.py:79
  116.6 91.3 %all-to-all-start = ((bf16[256,16,176]{0,2,1:T(8,128)(2,1)}), bf16[256,16,176]{0,2,1:T(8,128)(2,1)S(1)}, u32[]{:S(2)}, u32[]{:S(2)}) async-start(bf16[256,16,176]{0,2,1:T(8,128)(2,1)} %bitcast.3), calls=%async_computation | async-start | bytes 2883584 | tf_op jit(solution)/shard_map/all_to_all | solution.py:75
  129.2 87.2 %copy-start.1 = (bf16[16,22,8,256]{3,2,0,1:T(8,128)(2,1)S(1)}, bf16[16,22,8,256]{3,2,0,1:T(8,128)(2,1)}, u32[]{:S(2)}) copy-start(bf16[16,22,8,256]{3,2,0,1:T(8,128)(2,1)} %copy.41) | copy-start | bytes 4325380
  221.2 58.6 %copy-start.4 = (bf16[2816,256]{1,0:T(8,128)(2,1)S(1)}, bf16[2816,256]{1,0:T(8,128)(2,1)}, u32[]{:S(2)}) copy-start(bf16[2816,256]{1,0:T(8,128)(2,1)} %param.14) | copy-start | bytes 4325380
  222.0 8.6 %collective-permute-start = (bf16[176,512]{1,0:T(8,128)(2,1)S(1)}, bf16[176,512]{1,0:T(8,128)(2,1)S(1)}, u32[]{:S(2)}, u32[]{:S(2)}) collective-permute-start(bf16[176,512]{1,0:T(8,128)(2,1)S(1)} %fusion.12), channel_id=1, source_target_pairs={{0,32},{32,64},{64,96},{96,128},{128,160},{160,192},{192,224},{224... | collective-permute-start | bytes 540680 | tf_op jit(solution)/shard_map/ppermute | solution.py:23
  230.6 8.6 %collective-permute-start.1 = (bf16[176,512]{1,0:T(8,128)(2,1)S(1)}, bf16[176,512]{1,0:T(8,128)(2,1)S(1)}, u32[]{:S(2)}, u32[]{:S(2)}) collective-permute-start(bf16[176,512]{1,0:T(8,128)(2,1)S(1)} %collective-permute-done), channel_id=1, source_target_pairs={{0,32},{32,64},{64,96},{96,128},{128,160},{160,192},{192,224},{224... | collective-permute-start | bytes 540680 | tf_op jit(solution)/shard_map/ppermute | solution.py:23
  232.9 9.2 %collective-permute-start.8 = (bf16[176,512]{1,0:T(8,128)(2,1)S(1)}, bf16[176,512]{1,0:T(8,128)(2,1)S(1)}, u32[]{:S(2)}, u32[]{:S(2)}) collective-permute-start(bf16[176,512]{1,0:T(8,128)(2,1)S(1)} %fusion.12), channel_id=1, source_target_pairs={{32,0},{64,32},{96,64},{128,96},{160,128},{192,160},{224,192},{256... | collective-permute-start | bytes 540680 | tf_op jit(solution)/shard_map/ppermute | solution.py:25
  239.2 56.2 %copy-start.7 = (bf16[176,512]{1,0:T(8,128)(2,1)}, bf16[176,512]{1,0:T(8,128)(2,1)S(1)}, u32[]{:S(2)}) copy-start(bf16[176,512]{1,0:T(8,128)(2,1)S(1)} %collective-permute-done.1) | copy-start | bytes 540676
  239.2 9.4 %collective-permute-start.2 = (bf16[176,512]{1,0:T(8,128)(2,1)S(1)}, bf16[176,512]{1,0:T(8,128)(2,1)S(1)}, u32[]{:S(2)}, u32[]{:S(2)}) collective-permute-start(bf16[176,512]{1,0:T(8,128)(2,1)S(1)} %collective-permute-done.1), channel_id=1, source_target_pairs={{0,32},{32,64},{64,96},{96,128},{128,160},{160,192},{192,224},{224... | collective-permute-start | bytes 540680 | tf_op jit(solution)/shard_map/ppermute | solution.py:23
  242.0 53.4 %copy-start.5 = (bf16[176,512]{1,0:T(8,128)(2,1)}, bf16[176,512]{1,0:T(8,128)(2,1)S(1)}, u32[]{:S(2)}) copy-start(bf16[176,512]{1,0:T(8,128)(2,1)S(1)} %collective-permute-done.8) | copy-start | bytes 540676
  242.0 9.6 %collective-permute-start.9 = (bf16[176,512]{1,0:T(8,128)(2,1)S(1)}, bf16[176,512]{1,0:T(8,128)(2,1)S(1)}, u32[]{:S(2)}, u32[]{:S(2)}) collective-permute-start(bf16[176,512]{1,0:T(8,128)(2,1)S(1)} %collective-permute-done.8), channel_id=1, source_target_pairs={{32,0},{64,32},{96,64},{128,96},{160,128},{192,160},{224,192},{256... | collective-permute-start | bytes 540680 | tf_op jit(solution)/shard_map/ppermute | solution.py:25
  248.6 46.8 %copy-start.10 = (bf16[176,512]{1,0:T(8,128)(2,1)}, bf16[176,512]{1,0:T(8,128)(2,1)S(1)}, u32[]{:S(2)}) copy-start(bf16[176,512]{1,0:T(8,128)(2,1)S(1)} %collective-permute-done.2) | copy-start | bytes 540676
  248.6 10.5 %collective-permute-start.3 = (bf16[176,512]{1,0:T(8,128)(2,1)S(1)}, bf16[176,512]{1,0:T(8,128)(2,1)S(1)}, u32[]{:S(2)}, u32[]{:S(2)}) collective-permute-start(bf16[176,512]{1,0:T(8,128)(2,1)S(1)} %collective-permute-done.2), channel_id=1, source_target_pairs={{0,32},{32,64},{64,96},{96,128},{128,160},{160,192},{192,224},{224... | collective-permute-start | bytes 540680 | tf_op jit(solution)/shard_map/ppermute | solution.py:23
  251.6 43.8 %copy-start.8 = (bf16[176,512]{1,0:T(8,128)(2,1)}, bf16[176,512]{1,0:T(8,128)(2,1)S(1)}, u32[]{:S(2)}) copy-start(bf16[176,512]{1,0:T(8,128)(2,1)S(1)} %collective-permute-done.9) | copy-start | bytes 540676
  251.6 9.4 %collective-permute-start.10 = (bf16[176,512]{1,0:T(8,128)(2,1)S(1)}, bf16[176,512]{1,0:T(8,128)(2,1)S(1)}, u32[]{:S(2)}, u32[]{:S(2)}) collective-permute-start(bf16[176,512]{1,0:T(8,128)(2,1)S(1)} %collective-permute-done.9), channel_id=1, source_target_pairs={{32,0},{64,32},{96,64},{128,96},{160,128},{192,160},{224,192},{256... | collective-permute-start | bytes 540680 | tf_op jit(solution)/shard_map/ppermute | solution.py:25
  259.1 36.3 %copy-start.15 = (bf16[176,512]{1,0:T(8,128)(2,1)}, bf16[176,512]{1,0:T(8,128)(2,1)S(1)}, u32[]{:S(2)}) copy-start(bf16[176,512]{1,0:T(8,128)(2,1)S(1)} %collective-permute-done.3) | copy-start | bytes 540676
  259.1 9.7 %collective-permute-start.4 = (bf16[176,512]{1,0:T(8,128)(2,1)S(1)}, bf16[176,512]{1,0:T(8,128)(2,1)S(1)}, u32[]{:S(2)}, u32[]{:S(2)}) collective-permute-start(bf16[176,512]{1,0:T(8,128)(2,1)S(1)} %collective-permute-done.3), channel_id=1, source_target_pairs={{0,32},{32,64},{64,96},{96,128},{128,160},{160,192},{192,224},{224... | collective-permute-start | bytes 540680 | tf_op jit(solution)/shard_map/ppermute | solution.py:23
  261.0 34.4 %copy-start.11 = (bf16[176,512]{1,0:T(8,128)(2,1)}, bf16[176,512]{1,0:T(8,128)(2,1)S(1)}, u32[]{:S(2)}) copy-start(bf16[176,512]{1,0:T(8,128)(2,1)S(1)} %collective-permute-done.10) | copy-start | bytes 540676
  261.0 9.7 %collective-permute-start.11 = (bf16[176,512]{1,0:T(8,128)(2,1)S(1)}, bf16[176,512]{1,0:T(8,128)(2,1)S(1)}, u32[]{:S(2)}, u32[]{:S(2)}) collective-permute-start(bf16[176,512]{1,0:T(8,128)(2,1)S(1)} %collective-permute-done.10), channel_id=1, source_target_pairs={{32,0},{64,32},{96,64},{128,96},{160,128},{192,160},{224,192},{256... | collective-permute-start | bytes 540680 | tf_op jit(solution)/shard_map/ppermute | solution.py:25
  268.8 9.1 %collective-permute-start.5 = (bf16[176,512]{1,0:T(8,128)(2,1)S(1)}, bf16[176,512]{1,0:T(8,128)(2,1)}, u32[]{:S(2)}, u32[]{:S(2)}) collective-permute-start(bf16[176,512]{1,0:T(8,128)(2,1)S(1)} %collective-permute-done.4), channel_id=1, source_target_pairs={{0,32},{32,64},{64,96},{96,128},{128,160},{160,192},{192,224},{224... | collective-permute-start | bytes 540680 | tf_op jit(solution)/shard_map/ppermute | solution.py:23
  270.7 24.8 %copy-start.13 = (bf16[176,512]{1,0:T(8,128)(2,1)}, bf16[176,512]{1,0:T(8,128)(2,1)S(1)}, u32[]{:S(2)}) copy-start(bf16[176,512]{1,0:T(8,128)(2,1)S(1)} %collective-permute-done.11) | copy-start | bytes 540676
  270.7 10.8 %collective-permute-start.12 = (bf16[176,512]{1,0:T(8,128)(2,1)S(1)}, bf16[176,512]{1,0:T(8,128)(2,1)S(1)}, u32[]{:S(2)}, u32[]{:S(2)}) collective-permute-start(bf16[176,512]{1,0:T(8,128)(2,1)S(1)} %collective-permute-done.11), channel_id=1, source_target_pairs={{32,0},{64,32},{96,64},{128,96},{160,128},{192,160},{224,192},{256... | collective-permute-start | bytes 540680 | tf_op jit(solution)/shard_map/ppermute | solution.py:25
  277.9 8.9 %collective-permute-start.6 = (bf16[176,512]{1,0:T(8,128)(2,1)}, bf16[176,512]{1,0:T(8,128)(2,1)}, u32[]{:S(2)}, u32[]{:S(2)}) collective-permute-start(bf16[176,512]{1,0:T(8,128)(2,1)} %collective-permute-done.5), channel_id=1, source_target_pairs={{0,32},{32,64},{64,96},{96,128},{128,160},{160,192},{192,224},{224... | collective-permute-start | bytes 540680 | tf_op jit(solution)/shard_map/ppermute | solution.py:23
  281.5 13.9 %copy-start.16 = (bf16[176,512]{1,0:T(8,128)(2,1)}, bf16[176,512]{1,0:T(8,128)(2,1)S(1)}, u32[]{:S(2)}) copy-start(bf16[176,512]{1,0:T(8,128)(2,1)S(1)} %collective-permute-done.12) | copy-start | bytes 540676
  281.5 8.3 %collective-permute-start.13 = (bf16[176,512]{1,0:T(8,128)(2,1)S(1)}, bf16[176,512]{1,0:T(8,128)(2,1)S(1)}, u32[]{:S(2)}, u32[]{:S(2)}) collective-permute-start(bf16[176,512]{1,0:T(8,128)(2,1)S(1)} %collective-permute-done.12), channel_id=1, source_target_pairs={{32,0},{64,32},{96,64},{128,96},{160,128},{192,160},{224,192},{256... | collective-permute-start | bytes 540680 | tf_op jit(solution)/shard_map/ppermute | solution.py:25
  286.8 8.8 %collective-permute-start.7 = (bf16[176,512]{1,0:T(8,128)(2,1)}, bf16[176,512]{1,0:T(8,128)(2,1)S(1)}, u32[]{:S(2)}, u32[]{:S(2)}) collective-permute-start(bf16[176,512]{1,0:T(8,128)(2,1)} %collective-permute-done.6), channel_id=1, source_target_pairs={{0,32},{32,64},{64,96},{96,128},{128,160},{160,192},{192,224},{224... | collective-permute-start | bytes 540680 | tf_op jit(solution)/shard_map/ppermute | solution.py:23
  289.8 11.8 %collective-permute-start.14 = (bf16[176,512]{1,0:T(8,128)(2,1)S(1)}, bf16[176,512]{1,0:T(8,128)(2,1)S(1)}, u32[]{:S(2)}, u32[]{:S(2)}) collective-permute-start(bf16[176,512]{1,0:T(8,128)(2,1)S(1)} %collective-permute-done.13), channel_id=1, source_target_pairs={{32,0},{64,32},{96,64},{128,96},{160,128},{192,160},{224,192},{256... | collective-permute-start | bytes 540680 | tf_op jit(solution)/shard_map/ppermute | solution.py:25
  307.0 23.1 %copy-start.19 = (f32[256]{0:T(256)S(1)}, f32[256]{0:T(256)}, u32[]{:S(2)}) copy-start(f32[256]{0:T(256)} %param.15) | copy-start | bytes 3076
  320.1 26.2 %all-to-all-start.4 = ((f32[64,1,512]{2,1,0:T(1,128)}), f32[64,1,512]{2,1,0:T(1,128)S(1)}, u32[]{:S(2)}, u32[]{:S(2)}) async-start(f32[64,1,512]{2,1,0:T(1,128)} %broadcast_in_dim.7), calls=%async_computation.4 | async-start | bytes 262144 | tf_op jit(solution)/shard_map/all_to_all | solution.py:34
  (8 other events, 38.5 us)
Sparse Core Ops, SparseCore 0:
  44.1 172.2 all-gather.1
